TPU v7x, 32 devices: a whole 2x2x4 slice. The times are simulated.
32 devices in a mesh: tp: 16 (over z, y, core), dp: 2 (over x).
Axes of the slice: x: 2, y: 2, z: 4, core: 2. Of those that a mesh axis runs over, the one named last changes fastest.
Arguments:
- resid: bfloat16 [64, 2048], P('dp', 'tp'), may hold values from -6 to 6
- norm_gain: float32 [2, 2048], replicated, may hold values from 0.1 to 1.9
- w_query: bfloat16 [2, 2048, 2048], P(None, 'dp', 'tp'), may hold values from -0.125 to 0.125
- w_forget: bfloat16 [2, 2048, 2048], P(None, 'dp', 'tp'), may hold values from -0.125 to 0.125
- w_value: bfloat16 [2, 2048, 16, 128], P(None, 'dp', None, 'tp'), may hold values from -0.125 to 0.125
- w_gate: bfloat16 [2, 2048, 16, 128], P(None, 'dp', None, 'tp'), may hold values from -0.125 to 0.125
- gate_floor: float32 [2, 2048], replicated, may hold values from 0 to 0.9
- states: float32 [2, 64, 16, 128, 128], P(None, 'dp', None, 'tp'), may hold values from -1 to 1
- out_gain: float32 [2, 16, 128], P(None, None, 'tp'), may hold values from 0.1 to 1.9
- w_out: bfloat16 [2, 16, 128, 2048], P(None, None, 'tp'), may hold values from -0.125 to 0.125
Outputs:
- new_resid: bfloat16 [64, 2048], P('dp', 'tp')
- new_states: float32 [2, 64, 16, 128, 128], P(None, 'dp', None, 'tp')
All inputs are finite; a program needn't handle non-finite values.
Results may differ from a plain program's by a relative error of at most 0.029.
Values may be sent and summed in bfloat16 or wider, within the bound.
A program may use at most 64 MiB of HBM per device.

v0:
```python
import jax
import jax.numpy as jnp
from jax import lax
from jax.sharding import PartitionSpec as P

BLOCKS = 2


epsilon = 1e-06


def shards(
    resid, norm_gain, w_query, w_forget, w_value, w_gate, gate_floor, states, out_gain, w_out
):
    residual = resid
    seq_local = resid.shape[0]
    heads = states.shape[2]
    slice_cols = states.shape[3]
    head_dim = states.shape[4]
    row_count = w_query.shape[1]
    new_list = []
    for layer in range(BLOCKS):
        gathered = lax.all_gather(residual, "tp", axis=1, tiled=True)
        resid_f32 = gathered.astype(jnp.float32)
        inv_rms = lax.rsqrt(jnp.mean(resid_f32 * resid_f32, axis=1, keepdims=True) + epsilon)
        scaled = (resid_f32 * norm_gain[layer]).astype(jnp.bfloat16)
        query_rows = w_query[layer]
        forget_rows = w_forget[layer]
        value_rows = w_value[layer].reshape(row_count, -1)
        gate_rows = w_gate[layer].reshape(row_count, -1)
        zero_sums = (
            jnp.zeros((seq_local, query_rows.shape[1]), jnp.float32),
            jnp.zeros((seq_local, forget_rows.shape[1]), jnp.float32),
            jnp.zeros((seq_local, value_rows.shape[1]), jnp.float32),
            jnp.zeros((seq_local, gate_rows.shape[1]), jnp.float32),
        )
        totals = zero_sums
        pieces = (
            lax.all_gather(query_rows, "dp", axis=0, tiled=True),
            lax.all_gather(forget_rows, "dp", axis=0, tiled=True),
            lax.all_gather(value_rows, "dp", axis=0, tiled=True),
            lax.all_gather(gate_rows, "dp", axis=0, tiled=True),
        )
        segments = pieces[0].shape[0] // row_count
        for part_index in range(segments):
            columns = lax.dynamic_slice_in_dim(scaled, part_index * row_count, row_count, 1)
            lo_row = part_index * row_count
            totals = tuple(
                (
                    total
                    + lax.optimization_barrier(
                        jnp.dot(
                            columns,
                            segment[lo_row : lo_row + row_count],
                            preferred_element_type=jnp.float32,
                        ).astype(jnp.bfloat16)
                    ).astype(jnp.float32)
                    for total, segment in zip(totals, pieces)
                )
            )
        queries, forget_pre, values, gate_pre = [
            (summed * inv_rms).astype(jnp.bfloat16) for summed in totals
        ]
        query_all, forget_all = (
            lax.all_gather(queries, "tp", axis=1, tiled=True),
            lax.all_gather(forget_pre, "tp", axis=1, tiled=True),
        )
        floor_now = gate_floor[layer]
        keep = floor_now + (1.0 - floor_now) * jax.nn.sigmoid(forget_all.astype(jnp.float32))
        keep = keep.reshape(seq_local, heads, head_dim)
        value_f32 = values.astype(jnp.float32).reshape(seq_local, heads, slice_cols)
        state_new = (
            keep[:, :, None, :] * states[layer]
            + (1.0 - keep)[:, :, None, :] * value_f32[:, :, :, None]
        )
        query_f32 = query_all.astype(jnp.float32).reshape(seq_local, heads, head_dim)
        readout = jnp.sum(query_f32[:, :, None, :] * state_new, axis=3)
        power_sum = lax.psum(jnp.sum(readout * readout, axis=2), "tp")
        mean_square = power_sum[..., None] / head_dim
        gate_f32 = gate_pre.astype(jnp.float32).reshape(seq_local, heads, slice_cols)
        normed = (
            readout * lax.rsqrt(mean_square + epsilon) * out_gain[layer] * jax.nn.silu(gate_f32)
        ).astype(jnp.bfloat16)
        flattened = normed.reshape(seq_local, heads * slice_cols)
        weight_out = w_out[layer].reshape(heads * slice_cols, -1)
        branch = lax.psum_scatter(
            lax.dot_general(
                weight_out, flattened, (((0,), (1,)), ((), ())), preferred_element_type=jnp.float32
            ),
            "tp",
            scatter_dimension=0,
            tiled=True,
        )
        residual = (residual.astype(jnp.float32) + branch.T).astype(jnp.bfloat16)
        new_list.append(state_new)
    return (residual, jnp.stack(new_list))


def solution(mesh):
    return jax.shard_map(
        shards,
        mesh=mesh,
        in_specs=(
            P("dp", "tp"),
            P(),
            P(None, "dp", "tp"),
            P(None, "dp", "tp"),
            P(None, "dp", None, "tp"),
            P(None, "dp", None, "tp"),
            P(),
            P(None, "dp", None, "tp", None),
            P(None, None, "tp"),
            P(None, None, "tp", None),
        ),
        out_specs=(P("dp", "tp"), P(None, "dp", None, "tp", None)),
        check_vma=False,
    )
```

profile of v0, /device:TPU:0, one launch (start us, length us, event | category | flops | bytes accessed | tf_op | source)
XLA Modules:
  0.0 405.7 jit_solution(406525206643660046)
XLA Ops:
  7.2 0.8 fusion.65
  8.0 23.7 %all_gather.42 = bf16[32,2048]{1,0:T(8,128)(2,1)S(1)} all-gather(bf16[32,128]{1,0:T(8,128)(2,1)} %param.10), channel_id=1, replica_groups=mesh['tp'=16,'dp'=2] {'tp'}, dimensions={1}, use_global_device_ids=true | all-gather | bytes 139264 | tf_op jit(solution)/shard_map/all_gather | solution.py:23
  31.8 1.1 fusion.62
  32.8 9.4 %all-gather = bf16[1,2048,128]{2,1,0:T(8,128)(2,1)S(1)} all-gather(bf16[1,1024,128]{2,1,0:T(8,128)(2,1)S(1)} %get-tuple-element.7), channel_id=2, replica_groups=mesh['tp'=16,'dp'=2] {'dp'}, dimensions={1}, use_global_device_ids=true | all-gather | bytes 786432 | tf_op jit(solution)/shard_map/all_gather | solution.py:39
  42.3 0.2 convolution_convert_fusion.15
  42.5 0.2 convolution_convert_fusion.14
  42.7 8.5 %all-gather.1 = bf16[1,2048,128]{2,1,0:T(8,128)(2,1)S(1)} all-gather(bf16[1,1024,128]{2,1,0:T(8,128)(2,1)S(1)} %get-tuple-element.9), channel_id=3, replica_groups=mesh['tp'=16,'dp'=2] {'dp'}, dimensions={1}, use_global_device_ids=true | all-gather | bytes 786432 | tf_op jit(solution)/shard_map/all_gather | solution.py:40
  51.2 0.2 convolution_convert_fusion.13
  51.4 0.2 convolution_convert_fusion.12
  51.7 7.5 %all_gather.47 = bf16[2048,128]{0,1:T(8,128)(2,1)S(1)} all-gather(bf16[1024,128]{0,1:T(8,128)(2,1)S(1)} %get-tuple-element.10), channel_id=1, replica_groups=mesh['tp'=16,'dp'=2] {'dp'}, dimensions={0}, use_global_device_ids=true | all-gather | bytes 786432 | tf_op jit(solution)/shard_map/all_gather | solution.py:41
  59.2 0.2 convolution_convert_fusion.10
  59.3 0.2 convolution_convert_fusion.11
  59.6 7.0 %all_gather.48 = bf16[2048,128]{0,1:T(8,128)(2,1)S(1)} all-gather(bf16[1024,128]{0,1:T(8,128)(2,1)S(1)} %get-tuple-element.5), channel_id=1, replica_groups=mesh['tp'=16,'dp'=2] {'dp'}, dimensions={0}, use_global_device_ids=true | all-gather | bytes 786432 | tf_op jit(solution)/shard_map/all_gather | solution.py:42
  66.6 0.2 convolution_convert_fusion.8
  66.8 0.2 convolution_convert_fusion.9
  67.5 17.5 %all_gather.44 = bf16[32,2048]{1,0:T(8,128)(2,1)S(1)} all-gather(bf16[32,128]{1,0:T(8,128)(2,1)S(1)} %get-tuple-element.27), channel_id=1, replica_groups=mesh['tp'=16,'dp'=2] {'tp'}, dimensions={1}, use_global_device_ids=true | all-gather | bytes 139264 | tf_op jit(solution)/shard_map/all_gather | solution.py:65
  85.0 19.4 %all_gather.46 = bf16[32,2048]{1,0:T(8,128)(2,1)S(1)} all-gather(bf16[32,128]{1,0:T(8,128)(2,1)S(1)} %get-tuple-element.28), channel_id=1, replica_groups=mesh['tp'=16,'dp'=2] {'tp'}, dimensions={1}, use_global_device_ids=true | all-gather | bytes 139264 | tf_op jit(solution)/shard_map/all_gather | solution.py:66
  104.6 0.2 copy.25
  104.8 2.6 fusion.5
  107.6 57.8 %psum.14 = f32[32,16]{1,0:T(8,128)S(1)} all-reduce(f32[32,16]{1,0:T(8,128)S(1)} %multiply_reduce_fusion.1), channel_id=1, replica_groups=mesh['tp'=16,'dp'=2] {'tp'}, use_global_device_ids=true, to_apply=%region_3.0 | all-reduce | flops 512 | bytes 4096 | tf_op jit(solution)/shard_map/psum | solution.py:78
  165.6 0.2 copy.26
  165.8 1.0 convolution_bitcast_fusion.1
  167.0 9.5 %all-gather.2 = bf16[1,2048,128]{2,1,0:T(8,128)(2,1)} all-gather(bf16[1,1024,128]{2,1,0:T(8,128)(2,1)S(1)} %get-tuple-element.6), channel_id=4, replica_groups=mesh['tp'=16,'dp'=2] {'dp'}, dimensions={1}, use_global_device_ids=true | all-gather | bytes 786432 | tf_op jit(solution)/shard_map/all_gather | solution.py:39
  176.5 9.2 %all-gather.3 = bf16[1,2048,128]{2,1,0:T(8,128)(2,1)S(1)} all-gather(bf16[1,1024,128]{2,1,0:T(8,128)(2,1)S(1)} %get-tuple-element.8), channel_id=5, replica_groups=mesh['tp'=16,'dp'=2] {'dp'}, dimensions={1}, use_global_device_ids=true | all-gather | bytes 786432 | tf_op jit(solution)/shard_map/all_gather | solution.py:40
  185.7 8.4 %all_gather.54 = bf16[2048,128]{0,1:T(8,128)(2,1)} all-gather(bf16[1024,128]{0,1:T(8,128)(2,1)S(1)} %get-tuple-element.11), channel_id=1, replica_groups=mesh['tp'=16,'dp'=2] {'dp'}, dimensions={0}, use_global_device_ids=true | all-gather | bytes 786432 | tf_op jit(solution)/shard_map/all_gather | solution.py:41
  194.1 7.1 %all_gather.55 = bf16[2048,128]{0,1:T(8,128)(2,1)} all-gather(bf16[1024,128]{0,1:T(8,128)(2,1)S(1)} %get-tuple-element.4), channel_id=1, replica_groups=mesh['tp'=16,'dp'=2] {'dp'}, dimensions={0}, use_global_device_ids=true | all-gather | bytes 786432 | tf_op jit(solution)/shard_map/all_gather | solution.py:42
  201.3 18.7 %reduce-scatter.3.cloned.1.call-done = f32[128,32]{0,1:T(8,128)} async-done(((f32[2048,32]{0,1:T(8,128)}), f32[128,32]{0,1:T(8,128)}) %reduce-scatter.3.cloned.1.call-update) | async-done | bytes 16400 | tf_op jit(solution)/shard_map/reduce_scatter | solution.py:86
  220.0 0.7 fusion.47
  220.7 19.7 %all_gather.49 = bf16[32,2048]{1,0:T(8,128)(2,1)S(1)} all-gather(bf16[32,128]{1,0:T(8,128)(2,1)S(1)} %fusion.47), channel_id=1, replica_groups=mesh['tp'=16,'dp'=2] {'tp'}, dimensions={1}, use_global_device_ids=true | all-gather | bytes 139264 | tf_op jit(solution)/shard_map/all_gather | solution.py:23
  240.6 0.2 convolution_convert_fusion.5
  240.8 0.2 convolution_convert_fusion.4
  240.9 1.1 convolution_convert_fusion.3
  242.1 1.2 convolution_convert_fusion.2
  243.2 1.2 convolution_convert_fusion.1
  244.4 0.2 convolution_convert_fusion
  244.6 0.2 convolution_convert_fusion.6
  244.8 0.2 convolution_convert_fusion.7
  245.2 17.8 %all_gather.51 = bf16[32,2048]{1,0:T(8,128)(2,1)S(1)} all-gather(bf16[32,128]{1,0:T(8,128)(2,1)S(1)} %get-tuple-element.24), channel_id=1, replica_groups=mesh['tp'=16,'dp'=2] {'tp'}, dimensions={1}, use_global_device_ids=true | all-gather | bytes 139264 | tf_op jit(solution)/shard_map/all_gather | solution.py:65
  263.0 19.1 %all_gather.53 = bf16[32,2048]{1,0:T(8,128)(2,1)S(1)} all-gather(bf16[32,128]{1,0:T(8,128)(2,1)S(1)} %get-tuple-element.25), channel_id=1, replica_groups=mesh['tp'=16,'dp'=2] {'tp'}, dimensions={1}, use_global_device_ids=true | all-gather | bytes 139264 | tf_op jit(solution)/shard_map/all_gather | solution.py:66
  282.3 0.2 copy.30
  282.5 2.6 fusion.2
  285.2 57.8 %psum.15 = f32[32,16]{1,0:T(8,128)S(1)} all-reduce(f32[32,16]{1,0:T(8,128)S(1)} %multiply_reduce_fusion), channel_id=1, replica_groups=mesh['tp'=16,'dp'=2] {'tp'}, use_global_device_ids=true, to_apply=%region_8.9 | all-reduce | flops 512 | bytes 4096 | tf_op jit(solution)/shard_map/psum | solution.py:78
  343.2 0.2 copy.31
  343.4 1.0 convolution_bitcast_fusion
  344.4 3.5 multiply_add_fusion.1
  348.0 2.3 pad_maximum_fusion
  350.2 47.3 %reduce-scatter.5.cloned.1.call-done = f32[128,32]{0,1:T(8,128)} async-done(((f32[2048,32]{0,1:T(8,128)}), f32[128,32]{0,1:T(8,128)}) %reduce-scatter.5.cloned.1.call-update) | async-done | bytes 16400 | tf_op jit(solution)/shard_map/reduce_scatter | solution.py:86
  397.5 1.3 fusion.46
  (57 shorter events, 2.4 us)
Async XLA Ops:
  7.2 35.5 %copy-start.3 = (bf16[2,1024,128]{2,1,0:T(8,128)(2,1)S(1)}, bf16[2,1024,128]{2,1,0:T(8,128)(2,1)}, u32[]{:S(2)}) copy-start(bf16[2,1024,128]{2,1,0:T(8,128)(2,1)} %param.13) | copy-start | bytes 1572868
  7.2 212.8 %reduce-scatter.3.cloned.1.call-start = ((), (), s32[]{:S(2)}) async-start(), calls=%async_computation.2 | async-start | bytes 278528 | tf_op jit(solution)/shard_map/reduce_scatter | solution.py:86
  32.8 18.8 %copy-start.4 = (bf16[2,1024,16,8]{1,3,2,0:T(8,128)(2,1)S(1)}, bf16[2,1024,16,8]{1,3,2,0:T(8,128)(2,1)}, u32[]{:S(2)}) copy-start(bf16[2,1024,16,8]{1,3,2,0:T(8,128)(2,1)} %param.14) | copy-start | bytes 1572868
  42.7 16.8 %copy-start.5 = (bf16[2,1024,16,8]{1,3,2,0:T(8,128)(2,1)S(1)}, bf16[2,1024,16,8]{1,3,2,0:T(8,128)(2,1)}, u32[]{:S(2)}) copy-start(bf16[2,1024,16,8]{1,3,2,0:T(8,128)(2,1)} %param.15) | copy-start | bytes 1572868
  51.6 15.4 %copy-start.8 = (f32[2,16,8]{1,2,0:T(8,128)S(1)}, f32[2,16,8]{1,2,0:T(8,128)}, u32[]{:S(2)}) copy-start(f32[2,16,8]{1,2,0:T(8,128)} %param.18) | copy-start | bytes 3076
  51.6 15.6 %copy-start.7 = (f32[2,2048]{1,0:T(2,128)S(1)}, f32[2,2048]{1,0:T(2,128)}, u32[]{:S(2)}) copy-start(f32[2,2048]{1,0:T(2,128)} %param.16) | copy-start | bytes 49156
  104.8 61.0 %copy-start = (bf16[2,16,8,2048]{3,2,1,0:T(8,128)(2,1)S(1)}, bf16[2,16,8,2048]{3,2,1,0:T(8,128)(2,1)}, u32[]{:S(2)}) copy-start(bf16[2,16,8,2048]{3,2,1,0:T(8,128)(2,1)} %param.19) | copy-start | bytes 3145732
  165.8 54.2 %copy-start.6 = (bf16[32,128]{1,0:T(8,128)(2,1)S(1)}, bf16[32,128]{1,0:T(8,128)(2,1)}, u32[]{:S(2)}) copy-start(bf16[32,128]{1,0:T(8,128)(2,1)} %param.10) | copy-start | bytes 24580
  166.8 230.7 %reduce-scatter.5.cloned.1.call-start = ((), (), s32[]{:S(2)}) async-start(), calls=%async_computation.3 | async-start | bytes 278528 | tf_op jit(solution)/shard_map/reduce_scatter | solution.py:86
  185.7 58.9 %copy-start.1 = (bf16[1,2048,128]{2,1,0:T(8,128)(2,1)S(1)}, bf16[1,2048,128]{2,1,0:T(8,128)(2,1)}, u32[]{:S(2)}) copy-start(bf16[1,2048,128]{2,1,0:T(8,128)(2,1)} %all-gather.2) | copy-start | bytes 1572868
  201.3 43.1 %copy-start.2 = (bf16[2048,128]{0,1:T(8,128)(2,1)S(1)}, bf16[2048,128]{0,1:T(8,128)(2,1)}, u32[]{:S(2)}) copy-start(bf16[2048,128]{0,1:T(8,128)(2,1)} %all_gather.55) | copy-start | bytes 1572868
Sparse Core Ops, SparseCore 0:
  166.9 52.9 reduce-scatter.2
  344.5 52.9 reduce-scatter.4
where the time goes:
time: 406 us
  blocking collectives  300 us (74%)
  waiting for transfers between devices  66 us (16%)
  other arithmetic  14.4 us (4%)
  between operations  14.4 us (4%)
  matrix products  7.68 us (2%)
    psum x2, blocking collectives, shards(): power_sum = lax.psum(jnp.sum(readout * readout, axis=2), 'tp')  116 us
    reduce_scatter x2, waiting for transfers between devices, shards(): lax.psum_scatter(lax.dot_general(weight_out, flattened, (((0,), (1,)), ((...  66 us
    all_gather x2, blocking collectives, shards(): gathered = lax.all_gather(residual, 'tp', axis=1, tiled=True)  43.5 us
    all_gather x2, blocking collectives, shards(): lax.all_gather(forget_pre, 'tp', axis=1, tiled=True)  38.5 us
    all_gather x2, blocking collectives, shards(): lax.all_gather(queries, 'tp', axis=1, tiled=True)  35.3 us
    all_gather x2, blocking collectives, shards(): lax.all_gather(query_rows, 'dp', axis=0, tiled=True)  18.8 us
    all_gather x2, blocking collectives, shards(): lax.all_gather(forget_rows, 'dp', axis=0, tiled=True)  17.7 us
    all_gather x2, blocking collectives, shards(): lax.all_gather(value_rows, 'dp', axis=0, tiled=True)  15.9 us
  transfers between devices with their start and end apart: 2, of which 2 were waited for; matrix products, arithmetic and copies ran while one was open for 1% of the time, Pallas kernels for 0%

commit v1 on v0

--- a/solution.py
+++ b/solution.py
@@ -1,6 +1,10 @@
+import functools
+
 import jax
 import jax.numpy as jnp
 from jax import lax
+from jax.experimental import pallas as pl
+from jax.experimental.pallas import tpu as pltpu
 from jax.sharding import PartitionSpec as P
 
 BLOCKS = 2
@@ -96,9 +100,469 @@
     return (residual, jnp.stack(new_list))
 
 
+def fused_kernel(
+    n_tp,
+    n_dp,
+    resid_ref,
+    gain_ref,
+    floor_ref,
+    out_gain_ref,
+    wq_hbm,
+    wf_hbm,
+    wv_hbm,
+    wg_hbm,
+    wo_hbm,
+    states_hbm,
+    resid_out,
+    states_out,
+    wq,
+    wf,
+    wv,
+    wg,
+    wo,
+    st,
+    x_own,
+    x_all,
+    scaled,
+    part_out,
+    part_in,
+    ss_out,
+    ss_in,
+    qf_own,
+    qf_all,
+    q_f32,
+    keep_f32,
+    pw_own,
+    pw_all,
+    br_out,
+    br_in,
+    local_sem,
+    state_in_sem,
+    state_out_sem,
+    x_send,
+    x_recv,
+    p_send,
+    p_recv,
+    s_send,
+    s_recv,
+    q_send,
+    q_recv,
+    w_send,
+    w_recv,
+    b_send,
+    b_recv,
+):
+    me_t = lax.axis_index("tp")
+    me_d = lax.axis_index("dp")
+    seqs, cols = resid_ref.shape
+    heads, slice_cols, head_dim = st.shape[2:]
+    per_dp = n_tp // n_dp
+    width = n_tp * cols
+    blocks = wq.shape[0]
+    bf16, f32 = jnp.bfloat16, jnp.float32
+
+    weights = ((wq_hbm, wq), (wf_hbm, wf), (wv_hbm, wv), (wg_hbm, wg), (wo_hbm, wo))
+    weight_copies = [
+        [
+            pltpu.make_async_copy(src.at[layer], dst.at[layer], local_sem.at[layer, i])
+            for i, (src, dst) in enumerate(weights)
+        ]
+        for layer in range(blocks)
+    ]
+    state_copies = [
+        pltpu.make_async_copy(states_hbm.at[layer], st.at[layer], state_in_sem.at[layer])
+        for layer in range(blocks)
+    ]
+
+    barrier = pltpu.get_barrier_semaphore()
+
+    def greet(k, carry):
+        t = lax.rem(me_t + k // n_dp, n_tp)
+        d = lax.rem(me_d + k % n_dp, n_dp)
+        pl.semaphore_signal(barrier, inc=1, device_id={"tp": t, "dp": d})
+        return carry
+
+    lax.fori_loop(1, n_tp * n_dp, greet, 0)
+    for layer in range(blocks):
+        for copy in weight_copies[layer]:
+            copy.start()
+        state_copies[layer].start()
+    x_own[0] = resid_ref[...]
+
+    row_of = lax.broadcasted_iota(jnp.int32, (slice_cols, heads * slice_cols), 0)
+    col_of = lax.broadcasted_iota(jnp.int32, (slice_cols, heads * slice_cols), 1)
+    head_row = lax.broadcasted_iota(jnp.int32, (heads, heads * slice_cols), 0)
+    head_col = lax.broadcasted_iota(jnp.int32, (heads, heads * slice_cols), 1)
+    spread = (head_col // slice_cols == head_row).astype(f32)
+    gains = []
+    for layer in range(blocks):
+        wide = jnp.dot(
+            out_gain_ref[layer], spread, preferred_element_type=f32, precision=lax.Precision.HIGHEST
+        )
+        gains.append(
+            jnp.sum(jnp.where(col_of % slice_cols == row_of, wide, 0.0), axis=0, keepdims=True)
+        )
+
+    pl.semaphore_wait(barrier, n_tp * n_dp - 1)
+
+    group = seqs // 8
+    lanes = 128 // group
+    lane8 = lax.broadcasted_iota(jnp.int32, (8, 128), 1)
+    state_lane = lax.broadcasted_iota(jnp.int32, (heads, slice_cols, 128), 2)
+
+    for layer in range(blocks):
+        x_d = me_t // per_dp
+        x_j = me_t % per_dp
+
+        def x_copy(k):
+            return pltpu.make_async_remote_copy(
+                src_ref=x_own.at[layer],
+                dst_ref=x_all.at[layer, me_d, x_j],
+                send_sem=x_send.at[layer, k],
+                recv_sem=x_recv.at[layer, me_d, x_j],
+                device_id={"tp": lax.rem(me_t + k, n_tp), "dp": x_d},
+            )
+
+        def x_start(k, carry):
+            x_copy(k).start()
+            return carry
+
+        lax.fori_loop(1, n_tp, x_start, 0)
+
+        @pl.when(x_d != me_d)
+        def _():
+            x_copy(0).start()
+
+        @pl.when(x_d == me_d)
+        def _():
+            pltpu.make_async_copy(
+                x_own.at[layer], x_all.at[layer, me_d, x_j], x_recv.at[layer, me_d, x_j]
+            ).start()
+
+        squares = []
+        for d in range(n_dp):
+            total = jnp.zeros((seqs, cols), f32)
+            for j in range(per_dp):
+                pltpu.make_async_copy(
+                    x_own.at[layer], x_all.at[layer, d, j], x_recv.at[layer, d, j]
+                ).wait()
+                chunk = x_all[layer, d, j].astype(f32)
+                total = total + chunk * chunk
+                start = pl.multiple_of((me_d * per_dp + j) * cols, cols)
+                scaled[d * seqs : (d + 1) * seqs, j * cols : (j + 1) * cols] = (
+                    chunk * gain_ref[layer : layer + 1, pl.ds(start, cols)]
+                ).astype(bf16)
+            squares.append(jnp.sum(total, axis=1, keepdims=True))
+
+        for copy in weight_copies[layer]:
+            copy.wait()
+        xs = scaled[...]
+        nt = (((1,), (1,)), ((), ()))
+        parts = (
+            jnp.dot(xs, wq[layer], preferred_element_type=f32),
+            jnp.dot(xs, wf[layer], preferred_element_type=f32),
+            lax.dot_general(xs, wv[layer], nt, preferred_element_type=f32),
+            lax.dot_general(xs, wg[layer], nt, preferred_element_type=f32),
+        )
+        for d in range(n_dp):
+            for i in range(4):
+                part_out[layer, d, i] = parts[i][d * seqs : (d + 1) * seqs].astype(bf16)
+            tile = jnp.zeros((8, 128), f32)
+            for g in range(group):
+                tile = jnp.where(lane8 // lanes == g, squares[d][g * 8 : (g + 1) * 8], tile)
+            ss_out[layer, d] = tile
+
+        def p_copies(k):
+            peer = lax.rem(me_d + k, n_dp)
+            to = {"tp": me_t, "dp": peer}
+            return (
+                pltpu.make_async_remote_copy(
+                    src_ref=part_out.at[layer, peer],
+                    dst_ref=part_in.at[layer, me_d],
+                    send_sem=p_send.at[layer, k],
+                    recv_sem=p_recv.at[layer, me_d],
+                    device_id=to,
+                ),
+                pltpu.make_async_remote_copy(
+                    src_ref=ss_out.at[layer, peer],
+                    dst_ref=ss_in.at[layer, me_d],
+                    send_sem=s_send.at[layer, k],
+                    recv_sem=s_recv.at[layer, me_d],
+                    device_id=to,
+                ),
+            )
+
+        for k in range(1, n_dp):
+            for copy in p_copies(k):
+                copy.start()
+        sums = [part_out[layer, me_d, i].astype(f32) for i in range(4)]
+        square_tile = ss_out[layer, me_d]
+        for k in range(1, n_dp):
+            src = lax.rem(me_d + k, n_dp)
+            pltpu.make_async_copy(
+                part_out.at[layer, src], part_in.at[layer, src], p_recv.at[layer, src]
+            ).wait()
+            pltpu.make_async_copy(
+                ss_out.at[layer, src], ss_in.at[layer, src], s_recv.at[layer, src]
+            ).wait()
+            sums = [sums[i] + part_in[layer, src, i].astype(f32) for i in range(4)]
+            square_tile = square_tile + ss_in[layer, src]
+        inv_tile = lax.rsqrt(square_tile / width + epsilon)
+        inv_rms = jnp.concatenate(
+            [inv_tile[:, g * lanes : g * lanes + 1] for g in range(group)], axis=0
+        )
+        query, forget, value, gate = [(s * inv_rms).astype(bf16) for s in sums]
+        qf_own[layer, 0] = query
+        qf_own[layer, 1] = forget
+
+        def q_copy(k):
+            return pltpu.make_async_remote_copy(
+                src_ref=qf_own.at[layer],
+                dst_ref=qf_all.at[layer, me_t],
+                send_sem=q_send.at[layer, k],
+                recv_sem=q_recv.at[layer, me_t],
+                device_id={"tp": lax.rem(me_t + k, n_tp), "dp": me_d},
+            )
+
+        def q_start(k, carry):
+            q_copy(k).start()
+            return carry
+
+        lax.fori_loop(1, n_tp, q_start, 0)
+        qf_all[layer, me_t] = qf_own[layer]
+
+        value_t = jnp.transpose(
+            jnp.concatenate(
+                [value.astype(f32), jnp.zeros((128 - seqs, value.shape[1]), f32)], axis=0
+            )
+        ).reshape(heads, slice_cols, 128)
+        gate_f32 = gate.astype(f32)
+        gated = gains[layer] * (gate_f32 / (1.0 + jnp.exp(-gate_f32)))
+
+        def q_wait(k, carry):
+            src = lax.rem(me_t + n_tp - k, n_tp)
+            pltpu.make_async_copy(
+                qf_own.at[layer], qf_all.at[layer, src], q_recv.at[layer, src]
+            ).wait()
+            return carry
+
+        lax.fori_loop(1, n_tp, q_wait, 0)
+        for h in range(heads):
+            floor_now = floor_ref[layer : layer + 1, h * head_dim : (h + 1) * head_dim]
+            q_f32[h] = qf_all[layer, h, 0].astype(f32)
+            keep_f32[h] = floor_now + (1.0 - floor_now) * jax.nn.sigmoid(
+                qf_all[layer, h, 1].astype(f32)
+            )
+        state_copies[layer].wait()
+        readout = jnp.zeros((heads, slice_cols, 128), f32)
+        for s in range(seqs):
+            keep = keep_f32[:, s : s + 1, :]
+            new = keep * st[layer, s] + (1.0 - keep) * value_t[:, :, s : s + 1]
+            st[layer, s] = new
+            summed = jnp.sum(q_f32[:, s : s + 1, :] * new, axis=2, keepdims=True)
+            readout = jnp.where(state_lane == s, summed, readout)
+        pltpu.make_async_copy(st.at[layer], states_out.at[layer], state_out_sem.at[layer]).start()
+
+        power = jnp.sum(readout * readout, axis=1)
+        pw_own[layer] = power
+
+        def w_copy(k):
+            return pltpu.make_async_remote_copy(
+                src_ref=pw_own.at[layer],
+                dst_ref=pw_all.at[layer, me_t],
+                send_sem=w_send.at[layer, k],
+                recv_sem=w_recv.at[layer, me_t],
+                device_id={"tp": lax.rem(me_t + k, n_tp), "dp": me_d},
+            )
+
+        def w_start(k, carry):
+            w_copy(k).start()
+            return carry
+
+        lax.fori_loop(1, n_tp, w_start, 0)
+        pw_all[layer, me_t] = power
+
+        def w_wait(k, carry):
+            src = lax.rem(me_t + n_tp - k, n_tp)
+            pltpu.make_async_copy(
+                pw_own.at[layer], pw_all.at[layer, src], w_recv.at[layer, src]
+            ).wait()
+            return carry
+
+        lax.fori_loop(1, n_tp, w_wait, 0)
+        mean_square = jnp.sum(pw_all[layer], axis=0) / head_dim
+        unit = readout * lax.rsqrt(mean_square + epsilon)[:, None, :]
+        unit = jnp.transpose(unit.reshape(heads * slice_cols, 128))[:seqs]
+        normed = (unit * gated).astype(bf16)
+        for t in range(n_tp):
+            br_out[layer, t] = jnp.dot(
+                normed, wo[layer, :, t * cols : (t + 1) * cols], preferred_element_type=f32
+            ).astype(bf16)
+
+        def b_copy(k):
+            to = lax.rem(me_t + k, n_tp)
+            return pltpu.make_async_remote_copy(
+                src_ref=br_out.at[layer, to],
+                dst_ref=br_in.at[layer, me_t],
+                send_sem=b_send.at[layer, k],
+                recv_sem=b_recv.at[layer, me_t],
+                device_id={"tp": to, "dp": me_d},
+            )
+
+        def b_start(k, carry):
+            b_copy(k).start()
+            return carry
+
+        lax.fori_loop(1, n_tp, b_start, 0)
+        br_in[layer, me_t] = br_out[layer, me_t]
+
+        def b_wait(k, carry):
+            src = lax.rem(me_t + n_tp - k, n_tp)
+            pltpu.make_async_copy(
+                br_out.at[layer, src], br_in.at[layer, src], b_recv.at[layer, src]
+            ).wait()
+            return carry
+
+        lax.fori_loop(1, n_tp, b_wait, 0)
+        branch = jnp.sum(br_in[layer].astype(f32), axis=0)
+        new_resid = (x_own[layer].astype(f32) + branch).astype(bf16)
+        if layer + 1 < blocks:
+            x_own[layer + 1] = new_resid
+        else:
+            resid_out[...] = new_resid
+
+        @pl.when(x_d != me_d)
+        def _():
+            x_copy(0).wait_send()
+
+        def drain(k, carry):
+            x_copy(k).wait_send()
+            q_copy(k).wait_send()
+            w_copy(k).wait_send()
+            b_copy(k).wait_send()
+            return carry
+
+        lax.fori_loop(1, n_tp, drain, 0)
+        for k in range(1, n_dp):
+            for copy in p_copies(k):
+                copy.wait_send()
+
+    for layer in range(blocks):
+        pltpu.make_async_copy(st.at[layer], states_out.at[layer], state_out_sem.at[layer]).wait()
+
+
+def fused_shards(
+    n_tp,
+    n_dp,
+    resid,
+    norm_gain,
+    w_query,
+    w_forget,
+    w_value,
+    w_gate,
+    gate_floor,
+    states,
+    out_gain,
+    w_out,
+):
+    seqs, cols = resid.shape
+    blocks, _, heads, slice_cols, head_dim = states.shape
+    rows = w_query.shape[1]
+    local = heads * slice_cols
+    width = w_out.shape[3]
+    value_t = jnp.transpose(w_value, (0, 2, 3, 1)).reshape(blocks, local, rows)
+    gate_t = jnp.transpose(w_gate, (0, 2, 3, 1)).reshape(blocks, local, rows)
+    bf16, f32 = jnp.bfloat16, jnp.float32
+    dma = pltpu.SemaphoreType.DMA
+    vmem = pl.BlockSpec(memory_space=pltpu.VMEM)
+    hbm = pl.BlockSpec(memory_space=pl.ANY)
+    per_dp = n_tp // n_dp
+    return pl.pallas_call(
+        functools.partial(fused_kernel, n_tp, n_dp),
+        out_shape=(
+            jax.ShapeDtypeStruct(resid.shape, resid.dtype),
+            jax.ShapeDtypeStruct(states.shape, states.dtype),
+        ),
+        in_specs=[vmem] * 4 + [hbm] * 6,
+        out_specs=(vmem, hbm),
+        scratch_shapes=[
+            pltpu.VMEM(w_query.shape, bf16),
+            pltpu.VMEM(w_forget.shape, bf16),
+            pltpu.VMEM(value_t.shape, bf16),
+            pltpu.VMEM(gate_t.shape, bf16),
+            pltpu.VMEM((blocks, local, width), bf16),
+            pltpu.VMEM(states.shape, f32),
+            pltpu.VMEM((blocks, seqs, cols), bf16),
+            pltpu.VMEM((blocks, n_dp, per_dp, seqs, cols), bf16),
+            pltpu.VMEM((n_dp * seqs, rows), bf16),
+            pltpu.VMEM((blocks, n_dp, 4, seqs, cols), bf16),
+            pltpu.VMEM((blocks, n_dp, 4, seqs, cols), bf16),
+            pltpu.VMEM((blocks, n_dp, 8, 128), f32),
+            pltpu.VMEM((blocks, n_dp, 8, 128), f32),
+            pltpu.VMEM((blocks, 2, seqs, cols), bf16),
+            pltpu.VMEM((blocks, n_tp, 2, seqs, cols), bf16),
+            pltpu.VMEM((heads, seqs, head_dim), f32),
+            pltpu.VMEM((heads, seqs, head_dim), f32),
+            pltpu.VMEM((blocks, heads, 128), f32),
+            pltpu.VMEM((blocks, n_tp, heads, 128), f32),
+            pltpu.VMEM((blocks, n_tp, seqs, cols), bf16),
+            pltpu.VMEM((blocks, n_tp, seqs, cols), bf16),
+            dma((blocks, 5)),
+            dma((blocks,)),
+            dma((blocks,)),
+            dma((blocks, n_tp)),
+            dma((blocks, n_dp, per_dp)),
+            dma((blocks, n_dp)),
+            dma((blocks, n_dp)),
+            dma((blocks, n_dp)),
+            dma((blocks, n_dp)),
+            dma((blocks, n_tp)),
+            dma((blocks, n_tp)),
+            dma((blocks, n_tp)),
+            dma((blocks, n_tp)),
+            dma((blocks, n_tp)),
+            dma((blocks, n_tp)),
+        ],
+        compiler_params=pltpu.CompilerParams(
+            collective_id=0, has_side_effects=True, vmem_limit_bytes=56 * 1024 * 1024
+        ),
+    )(
+        resid,
+        norm_gain,
+        gate_floor,
+        jnp.transpose(out_gain, (0, 2, 1)),
+        w_query,
+        w_forget,
+        value_t,
+        gate_t,
+        w_out.reshape(blocks, local, width),
+        states,
+    )
+
+
+def choose(n_tp, n_dp, *args):
+    resid, w_query, states = args[0], args[2], args[7]
+    seqs, cols = resid.shape
+    _, _, heads, slice_cols, head_dim = states.shape
+    whole_tiles = (
+        cols == 128
+        and head_dim == 128
+        and heads == n_tp
+        and slice_cols == 8
+        and w_query.shape[2] == cols
+        and heads * slice_cols == cols
+        and n_tp % n_dp == 0
+        and seqs % 16 == 0
+        and seqs <= 128
+        and 1024 % seqs == 0
+    )
+    body = functools.partial(fused_shards, n_tp, n_dp) if whole_tiles else shards
+    return body(*args)
+
+
 def solution(mesh):
     return jax.shard_map(
-        shards,
+        functools.partial(choose, mesh.shape["tp"], mesh.shape["dp"]),
         mesh=mesh,
         in_specs=(
             P("dp", "tp"),

time: 406 us -> 75.7 us (0.19)
  blocking collectives: 300 us -> 0 us
  Pallas kernels: 0 us -> 68.7 us
  waiting for transfers between devices: 66 us -> 0 us
  other arithmetic: 14.4 us -> 0 us
  between operations: 14.4 us -> 0.64 us
  matrix products: 7.68 us -> 0 us
    all_gather x14 -> x0, blocking collectives: 184 us -> none  [the longest x2 43.5 us: shards(): gathered = lax.all_gather(residual, 'tp', axis=1, tiled=True)]
    psum x2 -> x0, blocking collectives: 116 us -> none  [shards(): power_sum = lax.psum(jnp.sum(readout * readout, axis=2), 'tp')]
    pallas_call x0 -> x1, Pallas kernels: none -> 68.7 us  [fused_shards(): pl.pallas_call(functools.partial(fused_kernel, n_tp, n_dp), out_shape=(ja...]
    reduce_scatter x2 -> x0, waiting for transfers between devices: 66 us -> none  [shards(): lax.psum_scatter(lax.dot_general(weight_out, flattened, (((0,), (1,)), ((...]
    dot_general x18 -> x0, matrix products: 7.68 us -> none  [the longest x16 5.69 us: shards(): jnp.dot(columns, segment[lo_row:lo_row + row_count], preferred_element_ty...]
    reduce_sum x6 -> x0, other arithmetic: 5.78 us -> none  [the longest x2 5.2 us: shards(): readout = jnp.sum(query_f32[:, :, None, :] * state_new, axis=3)]
    unnamed x22 -> x2, local copies, waits for them, and re-layouts: 0.29 us -> 5.99 us
  transfers between devices with their start and end apart: 2 -> 0, of which waited for: 2 -> 0; matrix products, arithmetic and copies ran while one was open for 1% -> 0% of each run, Pallas kernels for 0% -> 0%
where the time goes in v1:
time: 75.7 us; the launch traced here: 75.3 us
  Pallas kernels  68.7 us (91%)
  local copies, waits for them, and re-layouts  5.99 us (8%)
    pallas_call x1, Pallas kernels, fused_shards(): pl.pallas_call(functools.partial(fused_kernel, n_tp, n_dp), out_shape=(ja...  68.7 us
    unnamed x2, local copies, waits for them, and re-layouts  5.99 us

profile of v1, /device:TPU:0, one launch (start us, length us, event | category | flops | bytes accessed | tf_op | source)
XLA Modules:
  0.0 75.3 jit_solution(6114215540800534272)
XLA Ops:
  0.6 68.7 %shard_map.113 = (bf16[32,128]{1,0:T(8,128)(2,1)}, f32[2,32,16,8,128]{4,3,2,1,0:T(8,128)}) custom-call(bf16[32,128]{1,0:T(8,128)(2,1)} %resid_ref.1, f32[2,2048]{1,0:T(2,128)} %gain_ref.1, f32[2,2048]{1,0:T(2,128)} %floor_ref.1, f32[2,8,16]{2,1,0:T(8,128)} %bitcast.11, bf16[2,1024,128]{2,1,0:T(8,128)(2,1)} %wq_hbm.1, bf16[2,1024,128]{2,1,0:T(8,128)(2,1)} %wf_hbm.1, ...), custom_call_target="tpu_custom_call" | custom-call | tf_op jit(solution)/shard_map/pallas_call | solution.py:480
  69.3 1.3 %copy.14 = bf16[32,128]{1,0:T(8,128)(2,1)} copy(bf16[32,128]{1,0:T(8,128)(2,1)} %get-tuple-element.4) | data formatting | bytes 16384
  70.6 4.7 %copy.15 = f32[2,32,16,8,128]{4,3,2,1,0:T(8,128)} copy(f32[2,32,16,8,128]{4,3,2,1,0:T(8,128)} %get-tuple-element.5) | data formatting | bytes 8388608

commit v2 on v1

--- a/solution.py
+++ b/solution.py
@@ -114,13 +114,12 @@
     wo_hbm,
     states_hbm,
     resid_out,
-    states_out,
+    st,
     wq,
     wf,
     wv,
     wg,
     wo,
-    st,
     x_own,
     x_all,
     scaled,
@@ -132,13 +131,14 @@
     qf_all,
     q_f32,
     keep_f32,
+    v_cols,
+    reads,
     pw_own,
     pw_all,
     br_out,
     br_in,
     local_sem,
     state_in_sem,
-    state_out_sem,
     x_send,
     x_recv,
     p_send,
@@ -208,7 +208,11 @@
     group = seqs // 8
     lanes = 128 // group
     lane8 = lax.broadcasted_iota(jnp.int32, (8, 128), 1)
-    state_lane = lax.broadcasted_iota(jnp.int32, (heads, slice_cols, 128), 2)
+    row_lane = lax.broadcasted_iota(jnp.int32, (slice_cols, 128), 1)
+    heads_deep = heads * seqs // 128
+
+    def sent(sem, like):
+        pltpu.make_async_copy(like, like, sem).wait()
 
     for layer in range(blocks):
         x_d = me_t // per_dp
@@ -218,16 +222,13 @@
             return pltpu.make_async_remote_copy(
                 src_ref=x_own.at[layer],
                 dst_ref=x_all.at[layer, me_d, x_j],
-                send_sem=x_send.at[layer, k],
+                send_sem=x_send.at[layer],
                 recv_sem=x_recv.at[layer, me_d, x_j],
                 device_id={"tp": lax.rem(me_t + k, n_tp), "dp": x_d},
             )
 
-        def x_start(k, carry):
+        for k in range(1, n_tp):
             x_copy(k).start()
-            return carry
-
-        lax.fori_loop(1, n_tp, x_start, 0)
 
         @pl.when(x_d != me_d)
         def _():
@@ -239,6 +240,8 @@
                 x_own.at[layer], x_all.at[layer, me_d, x_j], x_recv.at[layer, me_d, x_j]
             ).start()
 
+        if layer > 0:
+            sent(b_send.at[layer - 1], br_out.at[layer - 1, 1:])
         squares = []
         for d in range(n_dp):
             total = jnp.zeros((seqs, cols), f32)
@@ -319,16 +322,13 @@
             return pltpu.make_async_remote_copy(
                 src_ref=qf_own.at[layer],
                 dst_ref=qf_all.at[layer, me_t],
-                send_sem=q_send.at[layer, k],
+                send_sem=q_send.at[layer],
                 recv_sem=q_recv.at[layer, me_t],
                 device_id={"tp": lax.rem(me_t + k, n_tp), "dp": me_d},
             )
 
-        def q_start(k, carry):
+        for k in range(1, n_tp):
             q_copy(k).start()
-            return carry
-
-        lax.fori_loop(1, n_tp, q_start, 0)
         qf_all[layer, me_t] = qf_own[layer]
 
         value_t = jnp.transpose(
@@ -339,60 +339,87 @@
         gate_f32 = gate.astype(f32)
         gated = gains[layer] * (gate_f32 / (1.0 + jnp.exp(-gate_f32)))
 
-        def q_wait(k, carry):
+        sent(x_send.at[layer], br_out.at[layer, 1:])
+
+        @pl.when(x_d != me_d)
+        def _():
+            sent(x_send.at[layer], br_out.at[layer, 0])
+
+        for k in range(1, n_dp):
+            for copy in p_copies(k):
+                copy.wait_send()
+        v_cols[...] = value_t
+        state_copies[layer].wait()
+
+        def one_head(h):
+            start = pl.multiple_of(h * head_dim, head_dim)
+            floor_now = floor_ref[layer : layer + 1, pl.ds(start, head_dim)]
+            q_f32[h] = qf_all[layer, h, 0].astype(f32)
+            keep_f32[h] = floor_now + (1.0 - floor_now) * jax.nn.sigmoid(
+                qf_all[layer, h, 1].astype(f32)
+            )
+            values_h = v_cols[h]
+            first = (h // heads_deep) * seqs
+            total = jnp.zeros((slice_cols, 128), f32)
+            for base in range(0, seqs, 8):
+                span = range(base, base + 8)
+                olds = [st[layer, s, h] for s in span]
+                keeps = [keep_f32[h, s : s + 1, :] for s in span]
+                queries = [q_f32[h, s : s + 1, :] for s in span]
+                news = [
+                    keeps[i] * olds[i] + (1.0 - keeps[i]) * values_h[:, s : s + 1]
+                    for i, s in enumerate(span)
+                ]
+                sums_h = [
+                    jnp.sum(queries[i] * news[i], axis=1, keepdims=True) for i in range(8)
+                ]
+                for i, s in enumerate(span):
+                    st[layer, s, h] = news[i]
+                    total = jnp.where(row_lane == first + s, sums_h[i], total)
+            reads[h] = total
+
+        one_head(me_t)
+
+        def far_head(k, carry):
             src = lax.rem(me_t + n_tp - k, n_tp)
             pltpu.make_async_copy(
                 qf_own.at[layer], qf_all.at[layer, src], q_recv.at[layer, src]
             ).wait()
+            one_head(src)
             return carry
 
-        lax.fori_loop(1, n_tp, q_wait, 0)
-        for h in range(heads):
-            floor_now = floor_ref[layer : layer + 1, h * head_dim : (h + 1) * head_dim]
-            q_f32[h] = qf_all[layer, h, 0].astype(f32)
-            keep_f32[h] = floor_now + (1.0 - floor_now) * jax.nn.sigmoid(
-                qf_all[layer, h, 1].astype(f32)
-            )
-        state_copies[layer].wait()
-        readout = jnp.zeros((heads, slice_cols, 128), f32)
-        for s in range(seqs):
-            keep = keep_f32[:, s : s + 1, :]
-            new = keep * st[layer, s] + (1.0 - keep) * value_t[:, :, s : s + 1]
-            st[layer, s] = new
-            summed = jnp.sum(q_f32[:, s : s + 1, :] * new, axis=2, keepdims=True)
-            readout = jnp.where(state_lane == s, summed, readout)
-        pltpu.make_async_copy(st.at[layer], states_out.at[layer], state_out_sem.at[layer]).start()
-
-        power = jnp.sum(readout * readout, axis=1)
+        lax.fori_loop(1, n_tp, far_head, 0)
+        readout = reads[...]
+        power = jnp.sum(
+            jnp.sum(readout * readout, axis=1).reshape(heads // heads_deep, heads_deep, 128), axis=0
+        )
         pw_own[layer] = power
 
         def w_copy(k):
             return pltpu.make_async_remote_copy(
                 src_ref=pw_own.at[layer],
                 dst_ref=pw_all.at[layer, me_t],
-                send_sem=w_send.at[layer, k],
-                recv_sem=w_recv.at[layer, me_t],
+                send_sem=w_send.at[layer],
+                recv_sem=w_recv.at[layer],
                 device_id={"tp": lax.rem(me_t + k, n_tp), "dp": me_d},
             )
 
-        def w_start(k, carry):
+        for k in range(1, n_tp):
             w_copy(k).start()
-            return carry
-
-        lax.fori_loop(1, n_tp, w_start, 0)
         pw_all[layer, me_t] = power
 
-        def w_wait(k, carry):
-            src = lax.rem(me_t + n_tp - k, n_tp)
-            pltpu.make_async_copy(
-                pw_own.at[layer], pw_all.at[layer, src], w_recv.at[layer, src]
-            ).wait()
-            return carry
-
-        lax.fori_loop(1, n_tp, w_wait, 0)
+        sent(q_send.at[layer], qf_all.at[layer, 1:])
+        pltpu.make_async_copy(
+            pw_all.at[layer, 1:], pw_all.at[layer, 1:], w_recv.at[layer]
+        ).wait()
         mean_square = jnp.sum(pw_all[layer], axis=0) / head_dim
-        unit = readout * lax.rsqrt(mean_square + epsilon)[:, None, :]
-        unit = jnp.transpose(unit.reshape(heads * slice_cols, 128))[:seqs]
+        folds = heads // heads_deep
+        unit = (
+            readout.reshape(folds, heads_deep, slice_cols, 128)
+            * lax.rsqrt(mean_square + epsilon)[None, :, None, :]
+        )
+        unit = jnp.transpose(unit.reshape(heads * slice_cols, 128))
+        unit = jnp.sum(unit.reshape(folds, seqs, heads * slice_cols), axis=0)
         normed = (unit * gated).astype(bf16)
         for t in range(n_tp):
             br_out[layer, t] = jnp.dot(
@@ -404,26 +431,19 @@
             return pltpu.make_async_remote_copy(
                 src_ref=br_out.at[layer, to],
                 dst_ref=br_in.at[layer, me_t],
-                send_sem=b_send.at[layer, k],
-                recv_sem=b_recv.at[layer, me_t],
+                send_sem=b_send.at[layer],
+                recv_sem=b_recv.at[layer],
                 device_id={"tp": to, "dp": me_d},
             )
 
-        def b_start(k, carry):
+        for k in range(1, n_tp):
             b_copy(k).start()
-            return carry
-
-        lax.fori_loop(1, n_tp, b_start, 0)
         br_in[layer, me_t] = br_out[layer, me_t]
 
-        def b_wait(k, carry):
-            src = lax.rem(me_t + n_tp - k, n_tp)
-            pltpu.make_async_copy(
-                br_out.at[layer, src], br_in.at[layer, src], b_recv.at[layer, src]
-            ).wait()
-            return carry
-
-        lax.fori_loop(1, n_tp, b_wait, 0)
+        sent(w_send.at[layer], pw_all.at[layer, 1:])
+        pltpu.make_async_copy(
+            br_in.at[layer, 1:], br_in.at[layer, 1:], b_recv.at[layer]
+        ).wait()
         branch = jnp.sum(br_in[layer].astype(f32), axis=0)
         new_resid = (x_own[layer].astype(f32) + branch).astype(bf16)
         if layer + 1 < blocks:
@@ -431,24 +451,7 @@
         else:
             resid_out[...] = new_resid
 
-        @pl.when(x_d != me_d)
-        def _():
-            x_copy(0).wait_send()
-
-        def drain(k, carry):
-            x_copy(k).wait_send()
-            q_copy(k).wait_send()
-            w_copy(k).wait_send()
-            b_copy(k).wait_send()
-            return carry
-
-        lax.fori_loop(1, n_tp, drain, 0)
-        for k in range(1, n_dp):
-            for copy in p_copies(k):
-                copy.wait_send()
-
-    for layer in range(blocks):
-        pltpu.make_async_copy(st.at[layer], states_out.at[layer], state_out_sem.at[layer]).wait()
+    sent(b_send.at[blocks - 1], br_out.at[blocks - 1, 1:])
 
 
 def fused_shards(
@@ -475,23 +478,22 @@
     bf16, f32 = jnp.bfloat16, jnp.float32
     dma = pltpu.SemaphoreType.DMA
     vmem = pl.BlockSpec(memory_space=pltpu.VMEM)
-    hbm = pl.BlockSpec(memory_space=pl.ANY)
+    hbm = pl.BlockSpec(memory_space=pltpu.HBM)
     per_dp = n_tp // n_dp
     return pl.pallas_call(
         functools.partial(fused_kernel, n_tp, n_dp),
         out_shape=(
-            jax.ShapeDtypeStruct(resid.shape, resid.dtype),
-            jax.ShapeDtypeStruct(states.shape, states.dtype),
+            pltpu.VMEM(resid.shape, resid.dtype),
+            pltpu.VMEM(states.shape, states.dtype),
         ),
         in_specs=[vmem] * 4 + [hbm] * 6,
-        out_specs=(vmem, hbm),
+        out_specs=(vmem, vmem),
         scratch_shapes=[
             pltpu.VMEM(w_query.shape, bf16),
             pltpu.VMEM(w_forget.shape, bf16),
             pltpu.VMEM(value_t.shape, bf16),
             pltpu.VMEM(gate_t.shape, bf16),
             pltpu.VMEM((blocks, local, width), bf16),
-            pltpu.VMEM(states.shape, f32),
             pltpu.VMEM((blocks, seqs, cols), bf16),
             pltpu.VMEM((blocks, n_dp, per_dp, seqs, cols), bf16),
             pltpu.VMEM((n_dp * seqs, rows), bf16),
@@ -503,25 +505,26 @@
             pltpu.VMEM((blocks, n_tp, 2, seqs, cols), bf16),
             pltpu.VMEM((heads, seqs, head_dim), f32),
             pltpu.VMEM((heads, seqs, head_dim), f32),
-            pltpu.VMEM((blocks, heads, 128), f32),
-            pltpu.VMEM((blocks, n_tp, heads, 128), f32),
+            pltpu.VMEM((heads, slice_cols, 128), f32),
+            pltpu.VMEM((heads, slice_cols, 128), f32),
+            pltpu.VMEM((blocks, heads * seqs // 128, 128), f32),
+            pltpu.VMEM((blocks, n_tp, heads * seqs // 128, 128), f32),
             pltpu.VMEM((blocks, n_tp, seqs, cols), bf16),
             pltpu.VMEM((blocks, n_tp, seqs, cols), bf16),
             dma((blocks, 5)),
             dma((blocks,)),
             dma((blocks,)),
-            dma((blocks, n_tp)),
             dma((blocks, n_dp, per_dp)),
             dma((blocks, n_dp)),
             dma((blocks, n_dp)),
             dma((blocks, n_dp)),
             dma((blocks, n_dp)),
+            dma((blocks,)),
             dma((blocks, n_tp)),
-            dma((blocks, n_tp)),
-            dma((blocks, n_tp)),
-            dma((blocks, n_tp)),
-            dma((blocks, n_tp)),
-            dma((blocks, n_tp)),
+            dma((blocks,)),
+            dma((blocks,)),
+            dma((blocks,)),
+            dma((blocks,)),
         ],
         compiler_params=pltpu.CompilerParams(
             collective_id=0, has_side_effects=True, vmem_limit_bytes=56 * 1024 * 1024
@@ -554,6 +557,8 @@
         and n_tp % n_dp == 0
         and seqs % 16 == 0
         and seqs <= 128
+        and heads * seqs % 128 == 0
+        and heads * seqs >= 128
         and 1024 % seqs == 0
     )
     body = functools.partial(fused_shards, n_tp, n_dp) if whole_tiles else shards

time: 75.7 us -> 66.9 us (0.88)
  Pallas kernels: 68.7 us -> 63.3 us
  local copies, waits for them, and re-layouts: 5.99 us -> 2.61 us
    pallas_call x1, Pallas kernels: 68.7 us -> 63.3 us  [fused_shards(): pl.pallas_call(functools.partial(fused_kernel, n_tp, n_dp), out_shape=(pl...]
    unnamed x2, local copies, waits for them, and re-layouts: 5.99 us -> 2.61 us
where the time goes in v2:
time: 66.9 us; the launch traced here: 66.6 us
  Pallas kernels  63.3 us (95%)
  local copies, waits for them, and re-layouts  2.61 us (4%)
    pallas_call x1, Pallas kernels, fused_shards(): pl.pallas_call(functools.partial(fused_kernel, n_tp, n_dp), out_shape=(pl...  63.3 us
    unnamed x2, local copies, waits for them, and re-layouts  2.61 us

profile of v2, /device:TPU:0, one launch (start us, length us, event | category | flops | bytes accessed | tf_op | source)
XLA Modules:
  0.0 66.6 jit_solution(14369164323895693575)
XLA Ops:
  0.6 63.3 %shard_map.113 = (bf16[32,128]{1,0:T(8,128)(2,1)S(1)}, f32[2,32,16,8,128]{4,3,2,1,0:T(8,128)S(1)}) custom-call(bf16[32,128]{1,0:T(8,128)(2,1)} %resid_ref.1, f32[2,2048]{1,0:T(2,128)} %gain_ref.1, f32[2,2048]{1,0:T(2,128)} %floor_ref.1, f32[2,8,16]{2,1,0:T(8,128)} %bitcast.11, bf16[2,1024,128]{2,1,0:T(8,128)(2,1)} %wq_hbm.1, bf16[2,1024,128]{2,1,0:T(8,128)(2,1)} %wf_hbm.1, ...), custom_call_target="tpu_custom_call" | custom-call | tf_op jit(solution)/shard_map/pallas_call | solution.py:483
  64.0 0.6 copy.14
  64.6 2.0 %copy.15 = f32[2,32,16,8,128]{4,3,2,1,0:T(8,128)} copy(f32[2,32,16,8,128]{4,3,2,1,0:T(8,128)S(1)} %get-tuple-element.3) | data formatting | bytes 8388608
